TPU v7x, 32 devices: a whole 2x2x4 slice. The times are simulated.
32 devices in a mesh: grp: 2 (over y), fs: 4 (over z), tp: 4 (over x, core).
Axes of the slice: x: 2, y: 2, z: 4, core: 2. Of those that a mesh axis runs over, the one named last changes fastest.
Arguments:
- tokens: bfloat16 [8192, 2048], P(('grp', 'fs')), parts along dimension 0, may hold values from -1300 to 1300
- norm_gain: bfloat16 [2048], replicated, may hold values from 0.099609375 to 1.8984375
- gate_weight: bfloat16 [2048, 5120], P('fs', 'tp'), may hold values from -0.125 to 0.125
- up_weight: bfloat16 [2048, 5120], P('fs', 'tp'), may hold values from -0.125 to 0.125
- down_weight: bfloat16 [5120, 2048], P('tp', 'fs'), may hold values from -0.078125 to 0.078125
Outputs:
- mixed: bfloat16 [8192, 2048], P(('grp', 'fs', 'tp')), parts along dimension 0
There are 2 independent parts, one for each index of `grp`. A program takes and returns all parts, laid end to end along the dimension named above; an argument that names none is the same for every part. Nothing has to cross between parts.
All inputs are finite; a program needn't handle non-finite values.
Results may differ from a plain program's by a relative error of at most 0.013.
Values may be sent and summed in bfloat16 or wider, within the bound.
A program may use at most 64 MiB of HBM per device.

v0:
```python
import jax
import jax.numpy as jnp
from jax import lax
from jax.sharding import PartitionSpec as P

EPSILON = 1e-06


def normalize(tokens, norm_gain):
    as_float = tokens.astype(jnp.float32)
    scale = lax.rsqrt(jnp.mean(as_float * as_float, axis=-1, keepdims=True) + EPSILON)
    return (as_float * scale * norm_gain.astype(jnp.float32)).astype(jnp.bfloat16)


def rounded(values):
    return lax.optimization_barrier(values.astype(jnp.bfloat16)).astype(jnp.float32)


def on_device(tokens, norm_gain, gate_weight, up_weight, down_weight):
    normed = normalize(tokens, norm_gain)
    gate_whole, up_whole = (
        lax.all_gather(gate_weight, "fs", axis=0, tiled=True),
        lax.all_gather(up_weight, "fs", axis=0, tiled=True),
    )
    gate_acts = jnp.dot(normed, gate_whole, preferred_element_type=jnp.float32)
    up_acts = jnp.dot(normed, up_whole, preferred_element_type=jnp.float32)
    hidden = (jax.nn.silu(gate_acts) * up_acts).astype(jnp.bfloat16)
    partials = rounded(
        jnp.dot(
            hidden,
            lax.all_gather(down_weight, "fs", axis=1, tiled=True),
            preferred_element_type=jnp.float32,
        )
    )
    mixed = lax.psum_scatter(partials.astype(jnp.bfloat16), "tp", scatter_dimension=0, tiled=True)
    return mixed


def solution(mesh):
    return jax.shard_map(
        on_device,
        mesh=mesh,
        in_specs=(P(("grp", "fs"), None), P(), P("fs", "tp"), P("fs", "tp"), P("tp", "fs")),
        out_specs=P(("grp", "fs", "tp"), None),
        check_vma=False,
    )
```

profile of v0, /device:TPU:0, one launch (start us, length us, event | category | flops | bytes accessed | tf_op | source)
XLA Modules:
  0.0 375.1 jit_solution(7898536820865071004)
XLA Ops:
  6.5 0.0 all-gather.4.cloned.1.call-start
  6.5 0.7 all-gather.4.cloned.1.call-update
  7.3 0.0 all-gather.6.cloned.1.call-start
  7.3 0.7 all-gather.6.cloned.1.call-update
  8.0 0.0 all-gather.8.cloned.1.call-start
  8.1 0.7 all-gather.8.cloned.1.call-update
  8.7 0.0 reduce-scatter.2.cloned.1.call-start
  8.8 0.7 convert_element_type.18
  9.5 3.1 fusion
  12.6 97.1 %all-gather.4.cloned.1.call-done = bf16[2048,1280]{1,0:T(8,128)(2,1)} async-done(((bf16[512,1280]{1,0:T(8,128)(2,1)}), bf16[2048,1280]{1,0:T(8,128)(2,1)}) %all-gather.4.cloned.1.call-update) | async-done | bytes 5242896 | tf_op jit(solution)/shard_map/all_gather | solution.py:22
  109.7 10.6 %fusion.4 = f32[1024,1280]{1,0:T(8,128)} fusion(bf16[2048,1280]{1,0:T(8,128)(2,1)} %all-gather.4.cloned.1.call-done, bf16[1024,2048]{1,0:T(8,128)(2,1)} %param.5, f32[2048]{0:T(1024)S(1)} %convert_element_type.18, f32[1024]{0:T(1024)S(1)} %add_rsqrt_fusion), kind=kOutput, calls=%fused_computation.7 | convolution fusion | flops 5377097728 | bytes 14692352 | tf_op jit(solution)/shard_map/dot_general | solution.py:25
  120.3 87.3 %all-gather.6.cloned.1.call-done = bf16[2048,1280]{1,0:T(8,128)(2,1)} async-done(((bf16[512,1280]{1,0:T(8,128)(2,1)}), bf16[2048,1280]{1,0:T(8,128)(2,1)}) %all-gather.6.cloned.1.call-update) | async-done | bytes 5242896 | tf_op jit(solution)/shard_map/all_gather | solution.py:23
  207.7 98.0 %all-gather.8.cloned.1.call-done = bf16[1280,2048]{1,0:T(8,128)(2,1)} async-done(((bf16[1280,512]{1,0:T(8,128)(2,1)}), bf16[1280,2048]{1,0:T(8,128)(2,1)}) %all-gather.8.cloned.1.call-update) | async-done | bytes 5242896 | tf_op jit(solution)/shard_map/all_gather | solution.py:31
  305.6 19.8 %convolution_convert_fusion = bf16[1024,2048]{1,0:T(8,128)(2,1)} fusion(bf16[1280,2048]{1,0:T(8,128)(2,1)} %all-gather.8.cloned.1.call-done, f32[1024,1280]{1,0:T(8,128)} %fusion.4, bf16[2048,1280]{1,0:T(8,128)(2,1)} %all-gather.6.cloned.1.call-done, bf16[1024,2048]{1,0:T(8,128)(2,1)} %param.5, f32[2048]{0:T(1024)S(1)} %convert_element_type.18, ...), kind=kOutput, calls=%fused_computation.6 | convolution fusion | flops 10755768320 | bytes 24129536 | tf_op jit(solution)/shard_map/dot_general | solution.py:29
  325.5 0.0 reduce-scatter.2.cloned.1.call-update
  325.5 43.0 %reduce-scatter.2.cloned.1.call-done = bf16[256,2048]{1,0:T(8,128)(2,1)} async-done(((bf16[1024,2048]{1,0:T(8,128)(2,1)}), bf16[256,2048]{1,0:T(8,128)(2,1)}) %reduce-scatter.2.cloned.1.call-update) | async-done | bytes 1048592 | tf_op jit(solution)/shard_map/reduce_scatter | solution.py:35
  (1 shorter events, 0.0 us)
Async XLA Ops:
  6.5 103.2 %all-gather.4.cloned.1.call-start = ((), (), s32[]{:S(2)}) async-start(), calls=%async_computation.1 | async-start | bytes 6553600 | tf_op jit(solution)/shard_map/all_gather | solution.py:22
  7.3 200.4 %all-gather.6.cloned.1.call-start = ((), (), s32[]{:S(2)}) async-start(), calls=%async_computation.2 | async-start | bytes 6553600 | tf_op jit(solution)/shard_map/all_gather | solution.py:23
  8.0 297.6 %all-gather.8.cloned.1.call-start = ((), (), s32[]{:S(2)}) async-start(), calls=%async_computation.3 | async-start | bytes 6553600 | tf_op jit(solution)/shard_map/all_gather | solution.py:31
  8.7 359.8 %reduce-scatter.2.cloned.1.call-start = ((), (), s32[]{:S(2)}) async-start(), calls=%async_computation.4 | async-start | bytes 5242880 | tf_op jit(solution)/shard_map/reduce_scatter | solution.py:35
Sparse Core Ops, SparseCore 0:
  8.9 100.7 all-gather.3
  111.3 96.3 all-gather.5
  209.2 96.3 all-gather.7
  325.6 42.8 reduce-scatter.1
where the time goes:
time: 375 us
  waiting for transfers between devices  328 us (87%)
  matrix products  30.5 us (8%)
  between operations  13.1 us (3%)
  other arithmetic  3.77 us (1%)
    all_gather x1, waiting for transfers between devices, on_device(): lax.all_gather(down_weight, 'fs', axis=1, tiled=True)  98 us
    all_gather x1, waiting for transfers between devices, on_device(): lax.all_gather(gate_weight, 'fs', axis=0, tiled=True)  97.1 us
    all_gather x1, waiting for transfers between devices, on_device(): lax.all_gather(up_weight, 'fs', axis=0, tiled=True)  87.3 us
    reduce_scatter x1, waiting for transfers between devices, on_device(): lax.psum_scatter(partials.astype(jnp.bfloat16), 'tp', scatter_dimension=0...  43 us
    dot_general x1, matrix products, on_device(): jnp.dot(hidden, lax.all_gather(down_weight, 'fs', axis=1, tiled=True), pr...  19.8 us
    dot_general x1, matrix products, on_device(): gate_acts = jnp.dot(normed, gate_whole, preferred_element_type=jnp.float32)  10.6 us
  transfers between devices with their start and end apart: 4, of which 4 were waited for; matrix products, arithmetic and copies ran while one was open for 4% of the time, Pallas kernels for 0%

commit v1 on v0

v1 whole, which is shorter than its diff:
```python
import functools

import jax
import jax.numpy as jnp
from jax import lax
from jax.experimental import pallas as pl
from jax.experimental.pallas import tpu as pltpu
from jax.sharding import PartitionSpec as P

EPSILON = 1e-06
MESH = pl.DeviceIdType.MESH
CORES = 2
VMEM_BYTES = 64 * 1024 * 1024 - 128 * 1024


def wrapped(value, size):
    return lax.rem(value, size)


def kernel(
    groups, n, chips, cuts,
    tok, gain, gu, dn, out,
    gbuf, dbuf, theirs, normed, hidden, keep, psend, precv, asend, arecv,
    gu_sent, gu_came, dn_sent, dn_came, tok_sent, tok_came, relay_sent, relay_came,
    pair_sent, pair_came, mix_sent, mix_came, local_sem,
):
    y, z, tp = lax.axis_index("grp"), lax.axis_index("fs"), lax.axis_index("tp")
    core, x = lax.rem(tp, CORES), lax.div(tp, CORES)
    partner = tp + 1 - 2 * core
    above, below = wrapped(z + 1, n), wrapped(z + n - 1, n)
    has_above, has_below = z < n - 1, z > 0

    rows, width = tok.shape
    depth, half = gu.shape[0], rows // 2
    units = dn.shape[0]
    columns = dn.shape[1]
    piece = depth // cuts
    own_rows = rows // (chips * CORES)
    peers = [(i, dx) for i in range(groups) for dx in range(chips) if (i, dx) != (0, 0)]

    def peer(i, dx):
        return wrapped(y + i, groups), wrapped(x + dx, chips)

    barrier = pltpu.get_barrier_semaphore()

    def greet(device):
        pl.semaphore_signal(barrier, inc=1, device_id=device, device_id_type=MESH)

    @pl.when(has_below)
    def _():
        greet({"fs": below})

    @pl.when(has_above)
    def _():
        greet({"fs": above})

    greet({"tp": partner})
    for i, dx in peers:
        g, xx = peer(i, dx)
        greet({"grp": g, "tp": CORES * xx + core})
    along_z = lax.div(z + n - 1, n) + lax.div(2 * n - 2 - z, n)
    pl.semaphore_wait(barrier, 1 + len(peers) + along_z)

    def gu_copy(slot, cut, direction, own=False):
        there = gbuf.at[pl.ds(pl.multiple_of(slot * depth + cut * piece, piece), piece)]
        index = slot * cuts + cut
        return pltpu.make_async_remote_copy(
            src_ref=gu.at[pl.ds(cut * piece, piece)] if own else there,
            dst_ref=there,
            send_sem=gu_sent.at[direction * n * cuts + index],
            recv_sem=gu_came.at[index],
            device_id={"fs": below if direction else above},
            device_id_type=MESH,
        )

    def dn_copy(slot, direction, own=False):
        return pltpu.make_async_remote_copy(
            src_ref=dn if own else dbuf.at[slot],
            dst_ref=dbuf.at[slot],
            send_sem=dn_sent.at[direction * n + slot],
            recv_sem=dn_came.at[slot],
            device_id={"fs": below if direction else above},
            device_id_type=MESH,
        )

    def tok_copy(i):
        part = pl.ds(pl.multiple_of(core * half, half), half)
        return pltpu.make_async_remote_copy(
            src_ref=tok.at[part],
            dst_ref=theirs.at[i - 1, part],
            send_sem=tok_sent.at[i - 1],
            recv_sem=tok_came.at[i - 1],
            device_id={"grp": wrapped(y + i, groups)},
            device_id_type=MESH,
        )

    def relay_copy(i):
        part = theirs.at[i - 1, pl.ds(pl.multiple_of(core * half, half), half)]
        return pltpu.make_async_remote_copy(
            src_ref=part,
            dst_ref=part,
            send_sem=relay_sent.at[i - 1],
            recv_sem=relay_came.at[i - 1],
            device_id={"tp": partner},
            device_id_type=MESH,
        )

    for cut in range(cuts):

        @pl.when(has_above)
        def _(cut=cut):
            gu_copy(z, cut, 0, own=True).start()

        @pl.when(has_below)
        def _(cut=cut):
            gu_copy(z, cut, 1, own=True).start()

    @pl.when(z == 0)
    def _():
        dn_copy(z, 0, own=True).start()

    @pl.when(z == n - 1)
    def _():
        dn_copy(z, 1, own=True).start()

    for i in range(1, groups):
        tok_copy(i).start()
    own_gu = pltpu.make_async_copy(
        gu, gbuf.at[pl.ds(pl.multiple_of(z * depth, depth), depth)], local_sem.at[0]
    )
    own_dn = pltpu.make_async_copy(dn, dbuf.at[z], local_sem.at[1])
    own_gu.start()
    own_dn.start()

    gains = gain[...].astype(jnp.float32)
    tile = 32

    def normalize(source, first):
        def step(t, carry):
            values = source[pl.ds(pl.multiple_of(t * tile, tile), tile), :].astype(jnp.float32)
            scale = lax.rsqrt(jnp.mean(values * values, axis=-1, keepdims=True) + EPSILON)
            normed[pl.ds(pl.multiple_of(first + t * tile, tile), tile), :] = (
                values * scale * gains
            ).astype(jnp.bfloat16)
            return carry

        lax.fori_loop(0, rows // tile, step, 0)

    normalize(tok, y * rows)

    def gather(s, carry):
        for cut in range(cuts):

            @pl.when(z >= s)
            def _(cut=cut):
                copy = gu_copy(z - s, cut, 0)
                copy.wait_recv()

                @pl.when(has_above)
                def _():
                    copy.start()

            @pl.when(z + s < n)
            def _(cut=cut):
                copy = gu_copy(z + s, cut, 1)
                copy.wait_recv()

                @pl.when(has_below)
                def _():
                    copy.start()

        @pl.when((s == z) & has_above)
        def _():
            dn_copy(z, 0, own=True).start()

        @pl.when((s == n - 1 - z) & has_below)
        def _():
            dn_copy(z, 1, own=True).start()

        return carry

    gather(1, 0)
    for i in range(1, groups):
        tok_copy(i).wait_recv()
        relay_copy(i).start()
    for i in range(1, groups):
        relay_copy(i).wait_recv()
        normalize(theirs.at[i - 1], wrapped(y + groups - i, groups) * rows)
    lax.fori_loop(2, n, gather, 0)
    own_gu.wait()
    own_dn.wait()

    tall = 512 if (groups * rows) % 512 == 0 else own_rows

    def activate(t, carry):
        where = pl.ds(pl.multiple_of(t * tall, tall), tall)
        mine = normed[where, :]
        gate_acts = jnp.dot(mine, gbuf[:, :units], preferred_element_type=jnp.float32)
        up_acts = jnp.dot(mine, gbuf[:, units:], preferred_element_type=jnp.float32)
        hidden[where, :] = (gate_acts / (1.0 + jnp.exp(-gate_acts)) * up_acts).astype(jnp.bfloat16)
        return carry

    lax.fori_loop(0, groups * rows // tall, activate, 0)

    def pair_copy(slot):
        return pltpu.make_async_remote_copy(
            src_ref=psend.at[slot],
            dst_ref=precv.at[slot],
            send_sem=pair_sent.at[slot],
            recv_sem=pair_came.at[slot],
            device_id={"tp": partner},
            device_id_type=MESH,
        )

    def mix_copy(slot, r):
        g, xx = peer(*peers[r])
        return pltpu.make_async_remote_copy(
            src_ref=asend.at[slot, g * chips + xx],
            dst_ref=arecv.at[slot, r],
            send_sem=mix_sent.at[slot * len(peers) + r],
            recv_sem=mix_came.at[slot * len(peers) + r],
            device_id={"grp": g, "tp": CORES * xx + core},
            device_id_type=MESH,
        )

    def product(slot, j, which):
        first = (CORES * j + which) * own_rows
        block = hidden[pl.ds(pl.multiple_of(first, own_rows), own_rows), :]
        return jnp.dot(block, dbuf[slot], preferred_element_type=jnp.float32)

    def block_of(slot):
        def give(j, carry):
            psend[slot, j] = product(slot, j, 1 - core).astype(jnp.bfloat16)
            return carry

        lax.fori_loop(0, groups * chips, give, 0)
        pair_copy(slot).start()

        def hold(j, carry):
            keep[j] = product(slot, j, core)
            return carry

        lax.fori_loop(0, groups * chips, hold, 0)
        pair_copy(slot).wait_recv()

        def add(j, carry):
            asend[slot, j] = (keep[j] + precv[slot, j].astype(jnp.float32)).astype(jnp.bfloat16)
            return carry

        lax.fori_loop(0, groups * chips, add, 0)
        for r in range(len(peers)):
            mix_copy(slot, r).start()

    def project(s, carry):
        @pl.when(z >= s)
        def _():
            copy = dn_copy(z - s, 0)
            copy.wait_recv()

            @pl.when(has_above)
            def _():
                copy.start()

            block_of(z - s)

        @pl.when(z + s < n)
        def _():
            copy = dn_copy(z + s, 1)
            copy.wait_recv()

            @pl.when(has_below)
            def _():
                copy.start()

            block_of(z + s)

        return carry

    block_of(z)
    lax.fori_loop(1, n, project, 0)

    def finish(slot):
        for r in range(len(peers)):
            mix_copy(slot, r).wait_recv()
        total = asend[slot, y * chips + x].astype(jnp.float32)
        for r in range(len(peers)):
            total = total + arecv[slot, r].astype(jnp.float32)
        out[:, pl.ds(pl.multiple_of(slot * columns, columns), columns)] = total.astype(jnp.bfloat16)

    def finish_step(s, carry):
        @pl.when(z >= s)
        def _():
            finish(z - s)

        @pl.when(z + s < n)
        def _():
            finish(z + s)

        return carry

    finish(z)
    lax.fori_loop(1, n, finish_step, 0)

    def left(slot, carry):
        @pl.when((slot <= z) & has_above)
        def _():
            for cut in range(cuts):
                gu_copy(slot, cut, 0).wait_send()
            dn_copy(slot, 0).wait_send()

        @pl.when((slot >= z) & has_below)
        def _():
            for cut in range(cuts):
                gu_copy(slot, cut, 1).wait_send()
            dn_copy(slot, 1).wait_send()

        pair_copy(slot).wait_send()
        for r in range(len(peers)):
            mix_copy(slot, r).wait_send()
        return carry

    lax.fori_loop(0, n, left, 0)
    for i in range(1, groups):
        tok_copy(i).wait_send()
        relay_copy(i).wait_send()


def on_device(groups, n, devices, tokens, norm_gain, gate_weight, up_weight, down_weight):
    chips, cuts = devices // CORES, 2
    rows, width = tokens.shape
    depth, columns = gate_weight.shape[0], down_weight.shape[1]
    share = gate_weight.shape[1] // groups
    units = -(-share // 128) * 128
    first = lax.axis_index("grp") * share

    def mine(weight, dim):
        part = lax.dynamic_slice_in_dim(weight, first, share, dim)
        short = [(0, units - share) if d == dim else (0, 0) for d in range(2)]
        return jnp.pad(part, short) if units > share else part

    gu = jnp.concatenate([mine(gate_weight, 1), mine(up_weight, 1)], axis=1)
    dn = mine(down_weight, 0)
    own_rows = rows // devices
    places, peers = groups * chips, groups * chips - 1
    bf16, f32, dma = jnp.bfloat16, jnp.float32, pltpu.SemaphoreType.DMA
    return pl.pallas_call(
        functools.partial(kernel, groups, n, chips, cuts),
        out_shape=jax.ShapeDtypeStruct((own_rows, width), bf16),
        in_specs=[pl.BlockSpec(memory_space=pltpu.VMEM)] * 4,
        out_specs=pl.BlockSpec(memory_space=pltpu.VMEM),
        scratch_shapes=[
            pltpu.VMEM((n * depth, 2 * units), bf16),
            pltpu.VMEM((n, units, columns), bf16),
            pltpu.VMEM((groups - 1, rows, width), bf16),
            pltpu.VMEM((groups * rows, width), bf16),
            pltpu.VMEM((groups * rows, units), bf16),
            pltpu.VMEM((places, own_rows, columns), f32),
            pltpu.VMEM((n, places, own_rows, columns), bf16),
            pltpu.VMEM((n, places, own_rows, columns), bf16),
            pltpu.VMEM((n, places, own_rows, columns), bf16),
            pltpu.VMEM((n, peers, own_rows, columns), bf16),
            dma((2 * n * cuts,)),
            dma((n * cuts,)),
            dma((2 * n,)),
            dma((n,)),
            dma((groups - 1,)),
            dma((groups - 1,)),
            dma((groups - 1,)),
            dma((groups - 1,)),
            dma((n,)),
            dma((n,)),
            dma((n * peers,)),
            dma((n * peers,)),
            dma((2,)),
        ],
        compiler_params=pltpu.CompilerParams(
            collective_id=0, has_side_effects=True, vmem_limit_bytes=VMEM_BYTES - 2**20
        ),
    )(tokens, norm_gain.reshape(1, width), gu, dn)


def solution(mesh):
    sizes = mesh.shape
    return jax.shard_map(
        functools.partial(on_device, sizes["grp"], sizes["fs"], sizes["tp"]),
        mesh=mesh,
        in_specs=(P(("grp", "fs"), None), P(), P("fs", "tp"), P("fs", "tp"), P("tp", "fs")),
        out_specs=P(("grp", "fs", "tp"), None),
        check_vma=False,
    )
```

time: 375 us -> 168 us (0.45)
  waiting for transfers between devices: 328 us -> 0 us
  Pallas kernels: 0 us -> 160 us
  matrix products: 30.5 us -> 0 us
  between operations: 13.1 us -> 0.02 us
  local copies, waits for them, and re-layouts: 0 us -> 5.8 us
    all_gather x3 -> x0, waiting for transfers between devices: 282 us -> none  [the longest x1 98 us: on_device(): lax.all_gather(down_weight, 'fs', axis=1, tiled=True)]
    pallas_call x0 -> x1, Pallas kernels: none -> 160 us  [on_device(): pl.pallas_call(functools.partial(kernel, groups, n, chips, cuts), out_sha...]
    reduce_scatter x1 -> x0, waiting for transfers between devices: 43 us -> none  [on_device(): lax.psum_scatter(partials.astype(jnp.bfloat16), 'tp', scatter_dimension=0...]
    dot_general x2 -> x0, matrix products: 30.5 us -> none  [the longest x1 19.8 us: on_device(): jnp.dot(hidden, lax.all_gather(down_weight, 'fs', axis=1, tiled=True), pr...]
  transfers between devices with their start and end apart: 4 -> 0, of which waited for: 4 -> 0; matrix products, arithmetic and copies ran while one was open for 4% -> 0% of each run, Pallas kernels for 0% -> 0%
where the time goes in v1:
time: 168 us; the launch traced here: 167 us
  Pallas kernels  160 us (95%)
  local copies, waits for them, and re-layouts  5.8 us (3%)
    pallas_call x1, Pallas kernels, on_device(): pl.pallas_call(functools.partial(kernel, groups, n, chips, cuts), out_sha...  160 us

profile of v1, /device:TPU:0, one launch (start us, length us, event | category | flops | bytes accessed | tf_op | source)
XLA Modules:
  0.0 167.4 jit_solution(9992144671435645519)
XLA Ops:
  0.0 1.4 constant_dynamic-slice_fusion.1
  1.4 0.0 copy-start
  1.4 1.2 pad_maximum_fusion.gu
  2.6 0.6 copy-done
  3.2 0.0 copy-start.1
  3.2 0.9 constant_dynamic-slice_fusion.dn
  4.1 0.0 copy-done.1
  4.1 0.6 reshape.3.gain
  4.7 160.4 %shard_map.55 = bf16[256,2048]{1,0:T(8,128)(2,1)} custom-call(bf16[1024,2048]{1,0:T(8,128)(2,1)} %tok.1, bf16[1,2048]{1,0:T(2,128)(2,1)} %reshape.3.gain, bf16[512,1280]{1,0:T(8,128)(2,1)} %pad_maximum_fusion.gu, bf16[640,512]{1,0:T(8,128)(2,1)} %constant_dynamic-slice_fusion.dn), custom_call_target="tpu_custom_call" | custom-call | tf_op jit(solution)/shard_map/pallas_call | solution.py:346
  165.1 2.3 %copy.7 = bf16[256,2048]{1,0:T(8,128)(2,1)} copy(bf16[256,2048]{1,0:T(8,128)(2,1)} %shard_map.55) | data formatting | bytes 2097152
Async XLA Ops:
  1.4 1.8 %copy-start = (bf16[1280,512]{1,0:T(8,128)(2,1)S(1)}, bf16[1280,512]{1,0:T(8,128)(2,1)}, u32[]{:S(2)}) copy-start(bf16[1280,512]{1,0:T(8,128)(2,1)} %param.9) | copy-start | bytes 3932164
  3.2 0.9 copy-start.1

commit v2 on v1

v2 whole, which is shorter than its diff:
```python
import functools

import jax
import jax.numpy as jnp
from jax import lax
from jax.experimental import pallas as pl
from jax.experimental.pallas import tpu as pltpu
from jax.sharding import PartitionSpec as P

EPSILON = 1e-06
MESH = pl.DeviceIdType.MESH
CORES = 2
VMEM_BYTES = 64 * 1024 * 1024 - 128 * 1024


def wrapped(value, size):
    return lax.rem(value, size)


def kernel(
    groups, n, chips, parts, sliced,
    tok, gain, gate, up, dn, out,
    gbuf, dbuf, raw, normed, acc, hidden, keep, psend, precv, asend, arecv,
    gu_sent, gu_came, dn_sent, dn_came, tok_sent, tok_came, relay_sent, relay_came,
    pair_sent, pair_came, mix_sent, mix_came, local_sem,
):
    y, z, tp = lax.axis_index("grp"), lax.axis_index("fs"), lax.axis_index("tp")
    core, x = lax.rem(tp, CORES), lax.div(tp, CORES)
    partner = tp + 1 - 2 * core
    above, below = wrapped(z + 1, n), wrapped(z + n - 1, n)
    has_above, has_below = z < n - 1, z > 0

    rows, width = tok.shape
    depth, half = gate.shape[0], rows // 2
    units = gbuf.shape[2]
    columns = dbuf.shape[2]
    own_rows = rows // (chips * CORES)
    first = 0 if sliced else pl.multiple_of(y * units, units)
    mine = (gate.at[:, pl.ds(first, units)], up.at[:, pl.ds(first, units)])
    places = groups * chips
    peers = [(i, dx) for i in range(groups) for dx in range(chips) if (i, dx) != (0, 0)]

    def peer(i, dx):
        return wrapped(y + i, groups), wrapped(x + dx, chips)

    def rows_of(slot):
        return pl.ds(pl.multiple_of(slot * depth, depth), depth)

    def own_dn(h):
        return dn.at[pl.ds(first, units), pl.ds(h * columns, columns)]

    locals_ = [pltpu.make_async_copy(tok, raw.at[0], local_sem.at[0])]
    for k in range(2):
        locals_.append(
            pltpu.make_async_copy(mine[k], gbuf.at[k, rows_of(z)], local_sem.at[1 + k])
        )
    for h in range(parts):
        locals_.append(
            pltpu.make_async_copy(own_dn(h), dbuf.at[z * parts + h], local_sem.at[3 + h])
        )
    for copy in locals_:
        copy.start()

    barrier = pltpu.get_barrier_semaphore()

    def greet(device):
        pl.semaphore_signal(barrier, inc=1, device_id=device, device_id_type=MESH)

    @pl.when(has_below)
    def _():
        greet({"fs": below})

    @pl.when(has_above)
    def _():
        greet({"fs": above})

    greet({"tp": partner})
    for i, dx in peers:
        g, xx = peer(i, dx)
        greet({"grp": g, "tp": CORES * xx + core})
    along_z = lax.div(z + n - 1, n) + lax.div(2 * n - 2 - z, n)
    pl.semaphore_wait(barrier, 1 + len(peers) + along_z)

    def gu_copy(slot, k, direction, own=False):
        there = gbuf.at[k, rows_of(slot)]
        index = slot * 2 + k
        return pltpu.make_async_remote_copy(
            src_ref=mine[k] if own else there,
            dst_ref=there,
            send_sem=gu_sent.at[direction * n * 2 + index],
            recv_sem=gu_came.at[index],
            device_id={"fs": below if direction else above},
            device_id_type=MESH,
        )

    def dn_copy(slot, h, direction, own=False):
        index = slot * parts + h
        return pltpu.make_async_remote_copy(
            src_ref=own_dn(h) if own else dbuf.at[index],
            dst_ref=dbuf.at[index],
            send_sem=dn_sent.at[direction * n * parts + index],
            recv_sem=dn_came.at[index],
            device_id={"fs": below if direction else above},
            device_id_type=MESH,
        )

    def start_own_dn(direction):
        for h in range(parts):
            dn_copy(z, h, direction, own=True).start()

    def tok_copy(i):
        part = pl.ds(pl.multiple_of(core * half, half), half)
        return pltpu.make_async_remote_copy(
            src_ref=tok.at[part],
            dst_ref=raw.at[i, part],
            send_sem=tok_sent.at[i - 1],
            recv_sem=tok_came.at[i - 1],
            device_id={"grp": wrapped(y + i, groups)},
            device_id_type=MESH,
        )

    def relay_copy(i):
        part = raw.at[i, pl.ds(pl.multiple_of(core * half, half), half)]
        return pltpu.make_async_remote_copy(
            src_ref=part,
            dst_ref=part,
            send_sem=relay_sent.at[i - 1],
            recv_sem=relay_came.at[i - 1],
            device_id={"tp": partner},
            device_id_type=MESH,
        )

    for k in range(2):

        @pl.when(has_above)
        def _(k=k):
            gu_copy(z, k, 0, own=True).start()

        @pl.when(has_below)
        def _(k=k):
            gu_copy(z, k, 1, own=True).start()

    for i in range(1, groups):
        tok_copy(i).start()

    @pl.when(z == 0)
    def _():
        start_own_dn(0)

    @pl.when(z == n - 1)
    def _():
        start_own_dn(1)

    gains = gain[...].astype(jnp.float32)
    tile = 32

    def normalize(i, first_row):
        def step(t, carry):
            where = pl.ds(pl.multiple_of(t * tile, tile), tile)
            values = raw[i, where, :].astype(jnp.float32)
            scale = lax.rsqrt(jnp.mean(values * values, axis=-1, keepdims=True) + EPSILON)
            normed[pl.ds(pl.multiple_of(first_row + t * tile, tile), tile), :] = (
                values * scale * gains
            ).astype(jnp.bfloat16)
            return carry

        lax.fori_loop(0, rows // tile, step, 0)

    for copy in locals_:
        copy.wait()
    normalize(0, y * rows)

    def gather(s):
        for k in range(2):

            @pl.when(z >= s)
            def _(k=k):
                copy = gu_copy(z - s, k, 0)
                copy.wait_recv()

                @pl.when(has_above)
                def _():
                    copy.start()

            @pl.when(z + s < n)
            def _(k=k):
                copy = gu_copy(z + s, k, 1)
                copy.wait_recv()

                @pl.when(has_below)
                def _():
                    copy.start()

        @pl.when((s == z) & has_above)
        def _():
            start_own_dn(0)

        @pl.when((s == n - 1 - z) & has_below)
        def _():
            start_own_dn(1)

    total_rows = groups * rows
    tall = 512 if total_rows % 512 == 0 else own_rows

    def term(slot, opening):
        some = pl.ds(pl.multiple_of(slot * depth, depth), depth)

        def step(t, carry):
            where = pl.ds(pl.multiple_of(t * tall, tall), tall)
            for k in range(2):
                value = jnp.dot(normed[where, some], gbuf[k, some, :], preferred_element_type=jnp.float32)
                if opening:
                    acc[k, where, :] = value
                else:
                    acc[k, where, :] += value
            return carry

        lax.fori_loop(0, total_rows // tall, step, 0)

    def terms(s):
        @pl.when(z >= s)
        def _():
            term(z - s, False)

        @pl.when(z + s < n)
        def _():
            term(z + s, False)

    gather(1)
    for i in range(1, groups):
        tok_copy(i).wait_recv()
        relay_copy(i).start()
    for i in range(1, groups):
        relay_copy(i).wait_recv()
        normalize(i, wrapped(y + groups - i, groups) * rows)
    term(z, True)
    if n > 2:
        gather(2)
    terms(1)
    if n > 2:
        terms(2)

    def later(s, carry):
        gather(s)
        terms(s)
        return carry

    lax.fori_loop(3, n, later, 0)

    def activate(t, carry):
        where = pl.ds(pl.multiple_of(t * tile, tile), tile)
        gate_acts = acc[0, where, :]
        hidden[where, :] = (gate_acts / (1.0 + jnp.exp(-gate_acts)) * acc[1, where, :]).astype(
            jnp.bfloat16
        )
        return carry

    lax.fori_loop(0, total_rows // tile, activate, 0)

    def pair_copy(slot):
        return pltpu.make_async_remote_copy(
            src_ref=psend.at[slot],
            dst_ref=precv.at[slot],
            send_sem=pair_sent.at[slot],
            recv_sem=pair_came.at[slot],
            device_id={"tp": partner},
            device_id_type=MESH,
        )

    def mix_copy(slot, r):
        g, xx = peer(*peers[r])
        return pltpu.make_async_remote_copy(
            src_ref=asend.at[slot, g * chips + xx],
            dst_ref=arecv.at[slot, r],
            send_sem=mix_sent.at[slot * len(peers) + r],
            recv_sem=mix_came.at[slot * len(peers) + r],
            device_id={"grp": g, "tp": CORES * xx + core},
            device_id_type=MESH,
        )

    def product(slot, j, which):
        first = (CORES * j + which) * own_rows
        block = hidden[pl.ds(pl.multiple_of(first, own_rows), own_rows), :]
        return jnp.dot(block, dbuf[slot], preferred_element_type=jnp.float32)

    def block_of(slot):
        def give(j, carry):
            psend[slot, j] = product(slot, j, 1 - core).astype(jnp.bfloat16)
            return carry

        lax.fori_loop(0, groups * chips, give, 0)
        pair_copy(slot).start()

        def hold(j, carry):
            keep[j] = product(slot, j, core)
            return carry

        lax.fori_loop(0, groups * chips, hold, 0)
        pair_copy(slot).wait_recv()

        def add(j, carry):
            asend[slot, j] = (keep[j] + precv[slot, j].astype(jnp.float32)).astype(jnp.bfloat16)
            return carry

        lax.fori_loop(0, groups * chips, add, 0)
        for r in range(len(peers)):
            mix_copy(slot, r).start()

    def project(s, carry):
        @pl.when(z >= s)
        def _():
            for h in range(parts):
                copy = dn_copy(z - s, h, 0)
                copy.wait_recv()

                @pl.when(has_above)
                def _():
                    copy.start()

                block_of((z - s) * parts + h)

        @pl.when(z + s < n)
        def _():
            for h in range(parts):
                copy = dn_copy(z + s, h, 1)
                copy.wait_recv()

                @pl.when(has_below)
                def _():
                    copy.start()

                block_of((z + s) * parts + h)

        return carry

    for h in range(parts):
        block_of(z * parts + h)
    lax.fori_loop(1, n, project, 0)

    def finish(slot):
        for r in range(len(peers)):
            mix_copy(slot, r).wait_recv()
        total = asend[slot, y * chips + x].astype(jnp.float32)
        for r in range(len(peers)):
            total = total + arecv[slot, r].astype(jnp.float32)
        out[:, pl.ds(pl.multiple_of(slot * columns, columns), columns)] = total.astype(jnp.bfloat16)

    def finish_step(s, carry):
        @pl.when(z >= s)
        def _():
            for h in range(parts):
                finish((z - s) * parts + h)

        @pl.when(z + s < n)
        def _():
            for h in range(parts):
                finish((z + s) * parts + h)

        return carry

    for h in range(parts):
        finish(z * parts + h)
    lax.fori_loop(1, n, finish_step, 0)

    def left(slot, carry):
        @pl.when((slot <= z) & has_above)
        def _():
            for k in range(2):
                gu_copy(slot, k, 0).wait_send()
            for h in range(parts):
                dn_copy(slot, h, 0).wait_send()

        @pl.when((slot >= z) & has_below)
        def _():
            for k in range(2):
                gu_copy(slot, k, 1).wait_send()
            for h in range(parts):
                dn_copy(slot, h, 1).wait_send()

        for h in range(parts):
            pair_copy(slot * parts + h).wait_send()
            for r in range(len(peers)):
                mix_copy(slot * parts + h, r).wait_send()
        return carry

    lax.fori_loop(0, n, left, 0)
    for i in range(1, groups):
        tok_copy(i).wait_send()
        relay_copy(i).wait_send()


def on_device(groups, n, devices, tokens, norm_gain, gate_weight, up_weight, down_weight):
    chips = devices // CORES
    rows, width = tokens.shape
    depth, columns = gate_weight.shape[0], down_weight.shape[1]
    parts = 2 if columns % 256 == 0 else 1
    columns //= parts
    share = gate_weight.shape[1] // groups
    units = -(-share // 128) * 128
    sliced = units > share
    if sliced:
        first = lax.axis_index("grp") * share

        def mine(weight, dim):
            part = lax.dynamic_slice_in_dim(weight, first, share, dim)
            return jnp.pad(part, [(0, units - share) if d == dim else (0, 0) for d in range(2)])

        gate_weight, up_weight = mine(gate_weight, 1), mine(up_weight, 1)
        down_weight = mine(down_weight, 0)
    own_rows = rows // devices
    places, peers, blocks = groups * chips, groups * chips - 1, n * parts
    bf16, f32, dma = jnp.bfloat16, jnp.float32, pltpu.SemaphoreType.DMA
    far, near = pl.BlockSpec(memory_space=pl.ANY), pl.BlockSpec(memory_space=pltpu.VMEM)
    return pl.pallas_call(
        functools.partial(kernel, groups, n, chips, parts, sliced),
        out_shape=jax.ShapeDtypeStruct((own_rows, width), bf16),
        in_specs=[far, near, far, far, far],
        out_specs=near,
        scratch_shapes=[
            pltpu.VMEM((2, n * depth, units), bf16),
            pltpu.VMEM((blocks, units, columns), bf16),
            pltpu.VMEM((groups, rows, width), bf16),
            pltpu.VMEM((groups * rows, width), bf16),
            pltpu.VMEM((2, groups * rows, units), f32),
            pltpu.VMEM((groups * rows, units), bf16),
            pltpu.VMEM((places, own_rows, columns), f32),
            pltpu.VMEM((blocks, places, own_rows, columns), bf16),
            pltpu.VMEM((blocks, places, own_rows, columns), bf16),
            pltpu.VMEM((blocks, places, own_rows, columns), bf16),
            pltpu.VMEM((blocks, peers, own_rows, columns), bf16),
            dma((2 * n * 2,)),
            dma((n * 2,)),
            dma((2 * blocks,)),
            dma((blocks,)),
            dma((groups - 1,)),
            dma((groups - 1,)),
            dma((groups - 1,)),
            dma((groups - 1,)),
            dma((blocks,)),
            dma((blocks,)),
            dma((blocks * peers,)),
            dma((blocks * peers,)),
            dma((3 + parts,)),
        ],
        compiler_params=pltpu.CompilerParams(
            collective_id=0, has_side_effects=True, vmem_limit_bytes=VMEM_BYTES - 2**20
        ),
    )(tokens, norm_gain.reshape(1, width), gate_weight, up_weight, down_weight)


def solution(mesh):
    sizes = mesh.shape
    return jax.shard_map(
        functools.partial(on_device, sizes["grp"], sizes["fs"], sizes["tp"]),
        mesh=mesh,
        in_specs=(P(("grp", "fs"), None), P(), P("fs", "tp"), P("fs", "tp"), P("tp", "fs")),
        out_specs=P(("grp", "fs", "tp"), None),
        check_vma=False,
    )
```

time: 168 us -> 156 us (0.929)
  Pallas kernels: 160 us -> 152 us
  local copies, waits for them, and re-layouts: 5.8 us -> 3.59 us
    pallas_call x1, Pallas kernels: 160 us -> 152 us  [on_device(): pl.pallas_call(functools.partial(kernel, groups, n, chips, parts, sliced)...]
    dynamic_slice x2 -> x0, local copies, waits for them, and re-layouts: 2.28 us -> none  [mine(): part = lax.dynamic_slice_in_dim(weight, first, share, dim)]
where the time goes in v2:
time: 156 us
  Pallas kernels  152 us (97%)
  local copies, waits for them, and re-layouts  3.59 us (2%)
    pallas_call x1, Pallas kernels, on_device(): pl.pallas_call(functools.partial(kernel, groups, n, chips, parts, sliced)...  152 us

profile of v2, /device:TPU:0, one launch (start us, length us, event | category | flops | bytes accessed | tf_op | source)
XLA Modules:
  0.0 155.6 jit_solution(3519691327034289175)
XLA Ops:
  0.0 1.3 reshape.3.gain
  1.3 152.0 %shard_map.55 = bf16[256,2048]{1,0:T(8,128)(2,1)} custom-call(bf16[1024,2048]{1,0:T(8,128)(2,1)} %tok.1, bf16[1,2048]{1,0:T(2,128)(2,1)} %reshape.3.gain, bf16[512,1280]{1,0:T(8,128)(2,1)} %gate.1, bf16[512,1280]{1,0:T(8,128)(2,1)} %up.1, bf16[1280,512]{1,0:T(8,128)(2,1)} %dn.1), custom_call_target="tpu_custom_call" | custom-call | tf_op jit(solution)/shard_map/pallas_call | solution.py:414
  153.3 2.3 %copy.7 = bf16[256,2048]{1,0:T(8,128)(2,1)} copy(bf16[256,2048]{1,0:T(8,128)(2,1)} %shard_map.55) | data formatting | bytes 2097152

commit v3 on v2

--- a/solution.py
+++ b/solution.py
@@ -170,8 +170,8 @@
         copy.wait()
     normalize(0, y * rows)
 
-    def gather(s):
-        for k in range(2):
+    def gather(s, kinds=(0, 1)):
+        for k in kinds:
 
             @pl.when(z >= s)
             def _(k=k):
@@ -191,6 +191,9 @@
                 def _():
                     copy.start()
 
+        if kinds[-1] == 0:
+            return
+
         @pl.when((s == z) & has_above)
         def _():
             start_own_dn(0)
@@ -202,12 +205,12 @@
     total_rows = groups * rows
     tall = 512 if total_rows % 512 == 0 else own_rows
 
-    def term(slot, opening):
+    def term(slot, opening, kinds=(0, 1)):
         some = pl.ds(pl.multiple_of(slot * depth, depth), depth)
 
         def step(t, carry):
             where = pl.ds(pl.multiple_of(t * tall, tall), tall)
-            for k in range(2):
+            for k in kinds:
                 value = jnp.dot(normed[where, some], gbuf[k, some, :], preferred_element_type=jnp.float32)
                 if opening:
                     acc[k, where, :] = value
@@ -217,14 +220,14 @@
 
         lax.fori_loop(0, total_rows // tall, step, 0)
 
-    def terms(s):
+    def terms(s, kinds=(0, 1)):
         @pl.when(z >= s)
         def _():
-            term(z - s, False)
+            term(z - s, False, kinds)
 
         @pl.when(z + s < n)
         def _():
-            term(z + s, False)
+            term(z + s, False, kinds)
 
     gather(1)
     for i in range(1, groups):
@@ -241,8 +244,9 @@
         terms(2)
 
     def later(s, carry):
-        gather(s)
-        terms(s)
+        for k in range(2):
+            gather(s, (k,))
+            terms(s, (k,))
         return carry
 
     lax.fori_loop(3, n, later, 0)
@@ -393,7 +397,7 @@
     chips = devices // CORES
     rows, width = tokens.shape
     depth, columns = gate_weight.shape[0], down_weight.shape[1]
-    parts = 2 if columns % 256 == 0 else 1
+    parts = 4 if columns % 512 == 0 else 1
     columns //= parts
     share = gate_weight.shape[1] // groups
     units = -(-share // 128) * 128

time: 156 us -> 155 us (level)
  no operation moved by 1% of the time
where the time goes in v3:
time: 155 us
  Pallas kernels  151 us (97%)
  local copies, waits for them, and re-layouts  3.59 us (2%)
    pallas_call x1, Pallas kernels, on_device(): pl.pallas_call(functools.partial(kernel, groups, n, chips, parts, sliced)...  151 us

profile of v3, /device:TPU:0, one launch (start us, length us, event | category | flops | bytes accessed | tf_op | source)
XLA Modules:
  0.0 154.9 jit_solution(8164466759992008133)
XLA Ops:
  0.0 1.3 reshape.3.gain
  1.3 151.3 %shard_map.55 = bf16[256,2048]{1,0:T(8,128)(2,1)} custom-call(bf16[1024,2048]{1,0:T(8,128)(2,1)} %tok.1, bf16[1,2048]{1,0:T(2,128)(2,1)} %reshape.3.gain, bf16[512,1280]{1,0:T(8,128)(2,1)} %gate.1, bf16[512,1280]{1,0:T(8,128)(2,1)} %up.1, bf16[1280,512]{1,0:T(8,128)(2,1)} %dn.1), custom_call_target="tpu_custom_call" | custom-call | tf_op jit(solution)/shard_map/pallas_call | solution.py:418
  152.6 2.3 %copy.7 = bf16[256,2048]{1,0:T(8,128)(2,1)} copy(bf16[256,2048]{1,0:T(8,128)(2,1)} %shard_map.55) | data formatting | bytes 2097152
